TPU v7x, 32 devices: a whole 2x2x4 slice. The times are simulated.
32 devices in a mesh: row: 16 (over z, y, x), col: 2 (over core).
Axes of the slice: x: 2, y: 2, z: 4, core: 2. Of those that a mesh axis runs over, the one named last changes fastest.
Arguments:
- tokens: bfloat16 [2, 3072, 2048], P('col', 'row'), may hold values from -6 to 6
- proj_in: bfloat16 [2048, 512], P('col'), may hold values from -0.125 to 0.125
- proj_out: bfloat16 [512, 2048], P(None, 'row'), may hold values from -0.25 to 0.25
Outputs:
- output: bfloat16 [2, 3072, 2048], P('col', 'row')
All inputs are finite; a program needn't handle non-finite values.
Results may differ from a plain program's by a relative error of at most 0.0083.
Values may be sent and summed in bfloat16 or wider, within the bound.
A program may use at most 64 MiB of HBM per device.

v0:
```python
import math

import jax
import jax.numpy as jnp
from jax import lax
from jax.sharding import PartitionSpec as P

GRP = 128


highest = lax.Precision.HIGHEST
span_inner = 128


def circle(height, breadth, period):
    product = lax.iota(jnp.int32, height)[:, None] * lax.iota(jnp.int32, breadth)[None, :] % period
    angle = product.astype(jnp.float32) * (2.0 * math.pi / period)
    return (jnp.cos(angle), jnp.sin(angle))


def positions(piece):
    real_in = piece[0, 0]
    imag_in = piece[1, 0]
    count, length = real_in.shape
    outer = length // span_inner
    real_in = real_in.reshape(count, outer, span_inner)
    imag_in = imag_in.reshape(count, outer, span_inner)
    cos_one, sin_one = circle(outer, outer, outer)
    first_re = jnp.einsum("ab,kbq->kaq", cos_one, real_in, precision=highest) - jnp.einsum(
        "ab,kbq->kaq", sin_one, imag_in, precision=highest
    )
    first_im = jnp.einsum("ab,kbq->kaq", sin_one, real_in, precision=highest) + jnp.einsum(
        "ab,kbq->kaq", cos_one, imag_in, precision=highest
    )
    twist_c, twist_s = circle(outer, span_inner, length)
    turned_re = first_re * twist_c - first_im * twist_s
    turned_im = first_re * twist_s + first_im * twist_c
    cos_two, sin_two = circle(span_inner, span_inner, span_inner)
    factor = 1.0 / math.sqrt(GRP * length)
    real_out = jnp.einsum("kaq,qb->kba", turned_re, cos_two, precision=highest) - jnp.einsum(
        "kaq,qb->kba", turned_im, sin_two, precision=highest
    )
    real_out = real_out.reshape(count, length) * factor
    return real_out[:, None, :]


def shards(tokens, proj_in, proj_out):
    seq_rows = tokens[0]
    local_len = seq_rows.shape[0]
    features = proj_in.shape[1]
    groups = features // GRP
    mapped = jnp.dot(
        seq_rows,
        lax.all_gather(proj_in, "col", axis=0, tiled=True),
        preferred_element_type=jnp.float32,
    ).astype(jnp.bfloat16)
    values = mapped.astype(jnp.float32).reshape(local_len, groups, GRP)
    cos_c, sin_c = circle(GRP, GRP, GRP)
    real_part = jnp.einsum("pgc,cs->gsp", values, cos_c, precision=highest)
    imag_part = jnp.einsum("pgc,cs->gsp", values, sin_c, precision=highest)
    ways = lax.axis_size("row")
    slots = groups * cos_c.shape[1]
    per_dev = slots // ways
    stacked = jnp.stack(
        [real_part.reshape(ways, per_dev, local_len), imag_part.reshape(ways, per_dev, local_len)],
        0,
    )
    spectra = positions(lax.all_to_all(stacked, "row", split_axis=1, concat_axis=3, tiled=True))
    outgoing = spectra.astype(jnp.bfloat16)
    back = lax.all_to_all(outgoing, "row", split_axis=2, concat_axis=0, tiled=True)
    mixed = back.reshape(features, local_len)
    result = lax.dot_general(
        mixed,
        lax.all_gather(proj_out, "row", axis=1, tiled=True),
        (((0,), (0,)), ((), ())),
        preferred_element_type=jnp.float32,
    )
    return result.astype(jnp.bfloat16)[None]


def solution(mesh):
    in_specs = (P("col", "row", None), P("col", None), P(None, "row"))
    out_specs = P("col", "row", None)
    return jax.shard_map(shards, mesh=mesh, in_specs=in_specs, out_specs=out_specs, check_vma=False)
```

profile of v0, /device:TPU:0, one launch (start us, length us, event | category | flops | bytes accessed | tf_op | source)
XLA Modules:
  0.0 115.2 jit_solution(4672272364211628046)
XLA Ops:
  6.5 0.0 copy-start
  6.5 0.0 all-gather.3.cloned.1.call-start
  6.5 0.7 all-gather.3.cloned.1.call-update
  7.3 0.0 all-gather.5.cloned.1.call-start
  7.3 0.7 all-gather.5.cloned.1.call-update
  8.0 14.2 %all-gather.3.cloned.1.call-done = bf16[2048,512]{1,0:T(8,128)(2,1)} async-done(((bf16[1024,512]{1,0:T(8,128)(2,1)}), bf16[2048,512]{1,0:T(8,128)(2,1)}) %all-gather.3.cloned.1.call-update) | async-done | bytes 2097168 | tf_op jit(solution)/shard_map/all_gather | solution.py:54
  22.2 0.0 copy-done
  22.2 2.2 %fusion.5 = bf16[24,4,8,128]{3,2,1,0:T(8,128)(2,1)S(1)} fusion(bf16[2048,512]{1,0:T(8,128)(2,1)} %all-gather.3.cloned.1.call-done, bf16[1,192,2048]{2,1,0:T(8,128)(2,1)S(1)} %copy-done), kind=kOutput, calls=%fused_computation.12 | convolution fusion | flops 402751488 | bytes 3080192 | tf_op jit(solution)/shard_map/dot_general | solution.py:52
  24.4 0.6 convolution_bitcast_fusion.1
  24.9 0.2 copy.19
  25.2 0.6 convolution_bitcast_fusion
  25.7 0.2 copy.21
  25.9 0.1 pad_maximum_fusion
  26.0 1.1 copy.22
  27.1 6.8 %all-to-all-start = ((f32[2,16,32,192]{3,2,0,1:T(8,128)}), f32[2,16,32,192]{3,2,0,1:T(8,128)S(1)}, u32[]{:S(2)}, u32[]{:S(2)}) async-start(f32[2,16,32,192]{3,2,0,1:T(8,128)} %copy.22), calls=%async_computation | async-start | bytes 2097152 | tf_op jit(solution)/shard_map/all_to_all | solution.py:68
  33.9 0.1 fusion.43
  34.0 24.7 %all-to-all-done = f32[2,16,32,192]{3,2,0,1:T(8,128)S(1)} async-done(((f32[2,16,32,192]{3,2,0,1:T(8,128)}), f32[2,16,32,192]{3,2,0,1:T(8,128)S(1)}, u32[]{:S(2)}, u32[]{:S(2)}) %all-to-all-start) | async-done | bytes 786464 | tf_op jit(solution)/shard_map/all_to_all | solution.py:68
  58.7 0.1 fusion.95
  58.8 0.3 copy.23
  59.1 0.3 reshape_squeeze.6
  59.4 0.3 copy.24
  59.7 0.3 reshape_squeeze.7
  60.0 0.5 fusion.39
  60.5 0.5 fusion.35
  61.0 0.5 fusion.2
  61.6 0.6 multiply_add_fusion
  62.2 0.7 fusion.9
  62.9 0.7 fusion.6
  63.7 0.4 copy.31
  64.1 0.4 reshape.66
  64.5 0.5 broadcast.106
  65.0 17.0 %reduce = bf16[3072,32]{1,0:T(8,128)(2,1)S(1)} reduce(bf16[3072,1,32]{2,1,0:T(2,128)(2,1)S(1)} %bitcast.68, bf16[]{:T(256)} %broadcast.106), dimensions={1}, to_apply=%bitcast.57.reduce_sub_computation | reduce | bytes 393218
  82.0 0.8 reshape.67
  82.7 19.8 %all_to_all.30 = bf16[16,2,3072]{2,1,0:T(2,128)(2,1)S(1)} all-to-all(bf16[16,2,3072]{2,1,0:T(2,128)(2,1)S(1)} %reshape.67), channel_id=1, replica_groups=mesh['row'=16,'col'=2] {'row'}, dimensions={0} | all-to-all | bytes 393216 | tf_op jit(solution)/shard_map/all_to_all | solution.py:70
  102.6 0.9 reshape.68
  103.4 1.4 %copy.29 = bf16[32,1,3072]{2,0,1:T(8,128)(2,1)S(1)} copy(bf16[32,1,3072]{0,1,2:T(2,128)(2,1)S(1)} %bitcast.69) | data formatting | bytes 393216 | tf_op jit(solution)/shard_map/all_to_all | solution.py:70
  104.8 0.3 all_to_all.26
  105.1 0.1 copy.30
  105.2 0.0 all-gather.5.cloned.1.call-done
  105.2 3.1 %fusion = bf16[1,192,2048]{2,1,0:T(8,128)(2,1)} fusion(bf16[512,192]{1,0:T(8,128)(2,1)S(1)} %bitcast.73, bf16[512,2048]{1,0:T(8,128)(2,1)} %all-gather.5.cloned.1.call-done), kind=kOutput, calls=%fused_computation.1 | convolution fusion | flops 403046400 | bytes 3080192 | tf_op jit(solution)/shard_map/dot_general | solution.py:72
Async XLA Ops:
  6.5 15.7 %copy-start = (bf16[1,192,2048]{2,1,0:T(8,128)(2,1)S(1)}, bf16[1,192,2048]{2,1,0:T(8,128)(2,1)}, u32[]{:S(2)}) copy-start(bf16[1,192,2048]{2,1,0:T(8,128)(2,1)} %param.3) | copy-start | bytes 2359300
  6.5 15.7 %all-gather.3.cloned.1.call-start = ((), (), s32[]{:S(2)}) async-start(), calls=%async_computation.2 | async-start | bytes 3145728 | tf_op jit(solution)/shard_map/all_gather | solution.py:54
  7.3 98.0 %all-gather.5.cloned.1.call-start = ((), (), s32[]{:S(2)}) async-start(), calls=%async_computation.3 | async-start | bytes 2228224 | tf_op jit(solution)/shard_map/all_gather | solution.py:74
  27.1 31.6 %all-to-all-start = ((f32[2,16,32,192]{3,2,0,1:T(8,128)}), f32[2,16,32,192]{3,2,0,1:T(8,128)S(1)}, u32[]{:S(2)}, u32[]{:S(2)}) async-start(f32[2,16,32,192]{3,2,0,1:T(8,128)} %copy.22), calls=%async_computation | async-start | bytes 2097152 | tf_op jit(solution)/shard_map/all_to_all | solution.py:68
Sparse Core Ops, SparseCore 0:
  8.9 13.2 all-gather.2
  24.9 73.4 all-gather.4
where the time goes:
time: 115 us
  waiting for transfers between devices  40.3 us (35%)
  blocking collectives  19.8 us (17%)
  other arithmetic  17.1 us (15%)
  between operations  13.6 us (12%)
  matrix products  10 us (9%)
  local copies, waits for them, and re-layouts  7.43 us (6%)
  starting transfers between devices  6.84 us (6%)
    all_to_all x1, waiting for transfers between devices, shards(): lax.all_to_all(stacked, 'row', split_axis=1, concat_axis=3, tiled=True)  24.7 us
    all_to_all x1, blocking collectives, shards(): lax.all_to_all(outgoing, 'row', split_axis=2, concat_axis=0, tiled=True)  19.8 us
    unnamed x1, other arithmetic  17 us
    all_gather x1, waiting for transfers between devices, shards(): lax.all_gather(proj_in, 'col', axis=0, tiled=True)  14.2 us
    all_to_all x1, starting transfers between devices, shards(): lax.all_to_all(stacked, 'row', split_axis=1, concat_axis=3, tiled=True)  6.8 us
    dot_general x1, matrix products, shards(): lax.dot_general(mixed, lax.all_gather(proj_out, 'row', axis=1, tiled=True...  3.08 us
  transfers between devices with their start and end apart: 3, of which 2 were waited for; matrix products, arithmetic and copies ran while one was open for 27% of the time, Pallas kernels for 0%

commit v1 on v0

--- a/solution.py
+++ b/solution.py
@@ -1,11 +1,17 @@
+import functools
 import math
 
 import jax
 import jax.numpy as jnp
+import numpy as np
 from jax import lax
+from jax.experimental import pallas as pl
+from jax.experimental.pallas import tpu as pltpu
 from jax.sharding import PartitionSpec as P
 
 GRP = 128
+LANES = 128
+TILE = 16
 
 
 highest = lax.Precision.HIGHEST
@@ -44,7 +50,7 @@
     return real_out[:, None, :]
 
 
-def shards(tokens, proj_in, proj_out):
+def plain(tokens, proj_in, proj_out):
     seq_rows = tokens[0]
     local_len = seq_rows.shape[0]
     features = proj_in.shape[1]
@@ -78,7 +84,402 @@
     return result.astype(jnp.bfloat16)[None]
 
 
+def tables(ways, local_len, groups):
+    slots = groups * GRP // ways
+    half = slots // 2
+    pack = LANES // slots
+    rows = local_len // pack
+    quads = ways // groups
+    length = ways * local_len
+
+    chan = np.arange(GRP)
+    freq = np.arange(GRP // 2).reshape(quads, half)
+    cos_part = np.cos(2 * np.pi * ((chan[:, None, None] * freq[None]) % GRP) / GRP)
+    sin_part = np.sin(2 * np.pi * ((chan[:, None, None] * freq[None]) % GRP) / GRP)
+    sin_part[:, 0, 0] = np.where(chan % 2 == 0, 1.0, -1.0)
+    both = np.stack([cos_part, sin_part], 2).reshape(GRP, quads, 1, slots)
+    spread = np.broadcast_to(both, (GRP, quads, pack, slots)).reshape(GRP, quads * LANES)
+
+    joint = np.zeros((quads, 2, half, GRP))
+    for quad in range(quads):
+        for at in range(half):
+            j = quad * half + at
+            if j == 0:
+                joint[quad, 0, at, 0] = 1.0
+                joint[quad, 1, at, GRP // 2] = 1.0
+            else:
+                joint[quad, 0, at, j] = 1.0
+                joint[quad, 1, at, j] = -1.0
+                joint[quad, 0, at, GRP - j] = 1.0
+                joint[quad, 1, at, GRP - j] = 1.0
+    joint = joint.reshape(quads, 1, slots, GRP)
+    gather = np.broadcast_to(joint, (quads, pack, slots, GRP)).reshape(quads * LANES, GRP)
+
+    part = np.arange(pack)[:, None, None]
+    dest = np.arange(ways)[None, :, None]
+    sub = np.arange(rows // ways)[None, None, :]
+    base = (dest * local_len + part * rows + sub * ways).reshape(-1, 1)
+    q = np.arange(local_len)[None, :]
+    factor = 1.0 / math.sqrt(GRP * length)
+    pieces = []
+    for a in range(ways // 2 + 1):
+        angle = 2 * np.pi * ((base + a) * q % length) / length
+        pieces.append(np.concatenate([np.cos(angle), -np.sin(angle)], 1))
+        if 0 < a < ways // 2:
+            angle = 2 * np.pi * ((base + ways - a) * q % length) / length
+            pieces.append(np.concatenate([np.cos(angle), np.sin(angle)], 1))
+    turn = np.concatenate(pieces, 0) * factor
+    return tuple(t.astype(jnp.bfloat16) for t in (spread, gather, turn))
+
+
+def scaled(x, factor):
+    return x if abs(factor - 1.0) < 1e-12 else x * factor
+
+
+def added(x, y):
+    return y if x is None else x if y is None else x + y
+
+
+def turned(re, im, cos, sin):
+    def term(value, factor):
+        return None if value is None or abs(factor) < 1e-12 else scaled(value, factor)
+
+    return (added(term(re, cos), term(im, -sin)), added(term(re, sin), term(im, cos)))
+
+
+def half_spectrum(xs):
+    n = len(xs)
+    if n == 1:
+        return [(xs[0], None)]
+    if n == 2:
+        return [(xs[0] + xs[1], None), (xs[0] - xs[1], None)]
+    even, odd = half_spectrum(xs[0::2]), half_spectrum(xs[1::2])
+    out = [None] * (n // 2 + 1)
+    for a in range(n // 4 + 1):
+        er, ei = even[a]
+        cos, sin = math.cos(2 * math.pi * a / n), math.sin(2 * math.pi * a / n)
+        tr, ti = turned(*odd[a], cos, sin)
+        minus = lambda v: None if v is None else -v
+        out[a] = (added(er, tr), added(ei, ti))
+        if n // 2 - a != a:
+            out[n // 2 - a] = (added(er, minus(tr)), added(minus(ei), ti))
+    return out
+
+
+def flipped(index, bit):
+    return index + bit - 2 * bit * ((index // bit) % 2)
+
+
+def kernel(
+    ways, cores, groups,
+    tok_h, pin_h, pout_h, spread_h, gather_h, turn_h, out_h,
+    tok, pin, wide, spread, gather, turn, acc, send1, recv1, spec, outer, send2, recv2, res,
+    load_sem, out_sem, pin_send, pin_recv, ex_send, ex_recv, ag_send, ag_recv, fw_send, fw_recv,
+):
+    row = lax.axis_index("row")
+    col = lax.axis_index("col")
+    local_len = tok.shape[1]
+    depth = pin_h.shape[0]
+    features = pin_h.shape[1]
+    width = pout_h.shape[1]
+    slots = features // ways
+    half = slots // 2
+    pack = LANES // slots
+    rows = local_len // pack
+    quads = ways // groups
+    share = features // cores
+
+    def core(m):
+        return lax.rem(col + m, cores)
+
+    loads = []
+
+    def load(src, dst):
+        copy = pltpu.make_async_copy(src, dst, load_sem.at[len(loads)])
+        copy.start()
+        loads.append(copy)
+        return copy
+
+    def own_columns(index):
+        return pl.ds(pl.multiple_of(index * width, LANES), width)
+
+    first = [load(pin_h, pin.at[0])]
+    for m in range(cores):
+        at = pl.ds(pl.multiple_of(core(m) * depth, LANES), depth)
+        copy = load(tok_h.at[0, :, at], tok.at[m])
+        if m == 0:
+            first.append(copy)
+        else:
+            later_tok = copy if m == 1 else later_tok
+    rest_tok = loads[2:]
+    own_out = load(pout_h, wide.at[:, own_columns(row)])
+    load_spread = load(spread_h, spread)
+    load_turn = load(turn_h, turn)
+    load_gather = load(gather_h, gather)
+
+    barrier = pltpu.get_barrier_semaphore()
+    for m in range(1, ways):
+        pl.semaphore_signal(barrier, inc=1, device_id={"row": lax.rem(row + m, ways)})
+    for m in range(1, cores):
+        pl.semaphore_signal(barrier, inc=1, device_id={"col": core(m)})
+
+    for copy in first:
+        copy.wait()
+    acc[...] = jnp.dot(tok[0], pin[0], preferred_element_type=jnp.float32)
+    own_out.wait()
+    pl.semaphore_wait(barrier, ways - 1 + cores - 1)
+
+    pin_copies = []
+    for m in range(1, cores):
+        copy = pltpu.make_async_remote_copy(
+            pin.at[0], pin.at[cores - m], pin_send.at[m - 1], pin_recv.at[cores - m - 1],
+            device_id={"col": core(m)},
+        )
+        copy.start()
+        pin_copies.append(copy)
+
+    bits = []
+    bit = ways // 2
+    while bit:
+        bits.append(bit)
+        bit //= 2
+    if len(bits) >= 2:
+        odd = lax.rem(col, 2)
+        bits = bits[:-2] + [1 + odd, 2 - odd]
+    blocks = [row]
+    my_rows = pl.ds(pl.multiple_of(col * share, TILE), share)
+    ag_copies = {}
+    fw_copies = []
+
+    def gather_step(step):
+        for at in range(2**step):
+            place = wide.at[my_rows, own_columns(blocks[at])]
+            slot = at + 2**step
+            copy = pltpu.make_async_remote_copy(
+                place, place, ag_send.at[slot], ag_recv.at[slot],
+                device_id={"row": flipped(row, bits[step])},
+            )
+            copy.start()
+            ag_copies[slot] = copy
+        blocks.extend([flipped(b, bits[step]) for b in blocks])
+
+    def gather_land(step):
+        for at in range(2**step, 2 ** (step + 1)):
+            ag_copies[at].wait_recv()
+            for m in range(1, cores):
+                place = wide.at[my_rows, own_columns(blocks[at])]
+                theirs = wide.at[
+                    pl.ds(pl.multiple_of(core(m) * share, TILE), share), own_columns(blocks_of(m)[at])
+                ]
+                put = pltpu.make_async_remote_copy(
+                    place, place, fw_send.at[at, m - 1], fw_recv.at[at, cores - m - 1],
+                    device_id={"col": core(m)},
+                )
+                put.start()
+                get = pltpu.make_async_remote_copy(
+                    theirs, theirs, fw_send.at[at, m - 1], fw_recv.at[at, m - 1],
+                    device_id={"col": core(m)},
+                )
+                fw_copies.append((put, get))
+
+    def blocks_of(m):
+        return blocks
+
+    steps = len(bits)
+    gather_step(0)
+
+    for copy in rest_tok[: cores - 1]:
+        copy.wait()
+    total = acc[...]
+    for m in range(1, cores):
+        pin_copies[cores - 1 - m].wait_recv()
+        total = total + jnp.dot(tok[m], pin[m], preferred_element_type=jnp.float32)
+    mapped = total.astype(jnp.bfloat16)
+    load_spread.wait()
+    lane_part = lax.broadcasted_iota(jnp.int32, (GRP, quads * LANES), 1) // slots % pack
+    table = spread[...]
+    table = jnp.concatenate(
+        [jnp.where(lane_part == t, table, jnp.zeros_like(table)) for t in range(pack)], 0
+    )
+    for g in range(groups):
+        cut = mapped[:, g * GRP : (g + 1) * GRP]
+        left = jnp.concatenate([cut[t * rows : (t + 1) * rows] for t in range(pack)], 1)
+        made = jnp.dot(left, table, preferred_element_type=jnp.float32).astype(jnp.bfloat16)
+        for quad in range(quads):
+            send1[g * quads + quad] = made[:, quad * LANES : (quad + 1) * LANES]
+
+    def exchange(src, dst, phase):
+        copies = []
+        for m in range(1, ways):
+            to = lax.rem(row + m, ways)
+            copy = pltpu.make_async_remote_copy(
+                src.at[to], dst.at[row], ex_send.at[phase, m], ex_recv.at[phase, m],
+                device_id={"row": to},
+            )
+            copy.start()
+            copies.append(copy)
+        dst[row] = src[row]
+        return copies
+
+    copies1 = exchange(send1, recv1, 0)
+    for step in range(steps - 2):
+        gather_land(step)
+        gather_step(step + 1)
+    for copy in copies1:
+        copy.wait_recv()
+    if steps >= 2:
+        gather_land(steps - 2)
+        gather_step(steps - 1)
+
+    lane = lax.broadcasted_iota(jnp.int32, (1, LANES), 1) % slots
+    lone = jnp.logical_and(lax.rem(row, quads) == 0, lane == half)
+    sine = jnp.logical_and(lane >= half, jnp.logical_not(lone))
+    sign = jnp.where(sine, -1.0, 1.0)
+    for strip in range(rows // TILE):
+        at = slice(strip * TILE, (strip + 1) * TILE)
+        xs = [recv1[r, at, :].astype(jnp.float32) for r in range(ways)]
+        for a, (re, im) in enumerate(half_spectrum(xs)):
+            im = jnp.zeros_like(re) if im is None else im
+            top = jnp.where(sine, im, re).astype(jnp.bfloat16)
+            low = jnp.where(sine, -re, im).astype(jnp.bfloat16)
+            for t in range(pack):
+                begin = t * rows + strip * TILE
+                spec[a, begin : begin + TILE, :] = top[:, t * slots : (t + 1) * slots]
+                begin += local_len
+                spec[a, begin : begin + TILE, :] = low[:, t * slots : (t + 1) * slots]
+    load_turn.wait()
+    begin = 0
+    for a in range(ways // 2 + 1):
+        single = a == 0 or 2 * a == ways
+        size = local_len if single else 2 * local_len
+        made = jnp.dot(turn[begin : begin + size], spec[a], preferred_element_type=jnp.float32)
+        begin += size
+        for at, which in enumerate([a] if single else [a, ways - a]):
+            piece = jnp.concatenate(
+                [made[at * local_len + t * rows : at * local_len + (t + 1) * rows] for t in range(pack)], 1
+            )
+            outer[pl.ds(which, rows, stride=ways), :] = piece if at == 0 else piece * sign
+    for r in range(ways):
+        send2[r] = outer[r * rows : (r + 1) * rows, :].astype(jnp.bfloat16)
+    copies2 = exchange(send2, recv2, 1)
+
+    load_gather.wait()
+    row_part = lax.broadcasted_iota(jnp.int32, (quads * LANES, GRP), 0) // slots % pack
+    table = gather[...]
+    table = jnp.concatenate(
+        [jnp.where(row_part == t, table, jnp.zeros_like(table)) for t in range(pack)], 1
+    )
+    for copy in copies2:
+        copy.wait_recv()
+    columns = []
+    for g in range(groups):
+        left = jnp.concatenate([recv2[g * quads + quad] for quad in range(quads)], 1)
+        made = jnp.dot(left, table, preferred_element_type=jnp.float32).astype(jnp.bfloat16)
+        columns.append(
+            jnp.concatenate([made[:, t * GRP : (t + 1) * GRP] for t in range(pack)], 0)
+        )
+    mixed = jnp.concatenate(columns, 1)
+    gather_land(steps - 1)
+    for _, get in fw_copies:
+        get.wait_recv()
+
+    model = wide.shape[1]
+    chunk = min(512, model)
+    stores = []
+    for at in range(model // chunk):
+        span = slice(at * chunk, (at + 1) * chunk)
+        res[:, span] = jnp.dot(mixed, wide[:, span], preferred_element_type=jnp.float32).astype(
+            jnp.bfloat16
+        )
+        copy = pltpu.make_async_copy(res.at[:, span], out_h.at[0, :, span], out_sem.at[at])
+        copy.start()
+        stores.append(copy)
+    for copy in copies1 + copies2 + pin_copies + list(ag_copies.values()):
+        copy.wait_send()
+    for put, _ in fw_copies:
+        put.wait_send()
+    for copy in stores:
+        copy.wait()
+
+
+def fused(ways, cores, tokens, proj_in, proj_out):
+    _, local_len, model = tokens.shape
+    depth, features = proj_in.shape
+    width = proj_out.shape[1]
+    groups = features // GRP
+    slots = features // ways
+    pack = LANES // slots
+    rows = local_len // pack
+    consts = [jnp.asarray(t) for t in tables(ways, local_len, groups)]
+    bf, f32 = jnp.bfloat16, jnp.float32
+    steps = ways
+    dma = pltpu.SemaphoreType.DMA
+    anywhere = pl.BlockSpec(memory_space=pl.ANY)
+    return pl.pallas_call(
+        functools.partial(kernel, ways, cores, groups),
+        out_shape=jax.ShapeDtypeStruct(tokens.shape, bf),
+        in_specs=[anywhere] * 6,
+        out_specs=anywhere,
+        scratch_shapes=[
+            pltpu.VMEM((cores, local_len, depth), bf),
+            pltpu.VMEM((cores, depth, features), bf),
+            pltpu.VMEM((features, model), bf),
+            pltpu.VMEM(consts[0].shape, bf),
+            pltpu.VMEM(consts[1].shape, bf),
+            pltpu.VMEM(consts[2].shape, bf),
+            pltpu.VMEM((local_len, features), f32),
+            pltpu.VMEM((ways, rows, LANES), bf),
+            pltpu.VMEM((ways, rows, LANES), bf),
+            pltpu.VMEM((ways // 2 + 1, 2 * local_len, slots), bf),
+            pltpu.VMEM((ways * rows, LANES), f32),
+            pltpu.VMEM((ways, rows, LANES), bf),
+            pltpu.VMEM((ways, rows, LANES), bf),
+            pltpu.VMEM((local_len, model), bf),
+            dma((cores + 5,)),
+            dma((max(1, model // 512),)),
+            dma((cores,)),
+            dma((cores,)),
+            dma((2, ways)),
+            dma((2, ways)),
+            dma((ways,)),
+            dma((ways,)),
+            dma((ways, cores)),
+            dma((ways, cores)),
+        ],
+        compiler_params=pltpu.CompilerParams(
+            collective_id=0, has_side_effects=True, vmem_limit_bytes=48 * 2**20
+        ),
+    )(tokens, proj_in, proj_out, *consts)
+
+
+def shards(ways, cores, tokens, proj_in, proj_out):
+    _, local_len, model = tokens.shape
+    depth, features = proj_in.shape
+    width = proj_out.shape[1]
+    groups = features // GRP
+    slots = max(1, features // ways)
+    pack = max(1, LANES // slots)
+    fits = (
+        ways >= 4
+        and ways & (ways - 1) == 0
+        and ways % groups == 0
+        and slots * pack == LANES
+        and slots % 2 == 0
+        and cores == 2
+        and local_len % pack == 0
+        and (local_len // pack) % max(ways, TILE) == 0
+        and width % LANES == 0
+        and depth % LANES == 0
+        and model % 512 == 0
+        and features % (cores * TILE) == 0
+    )
+    if fits:
+        return fused(ways, cores, tokens, proj_in, proj_out)
+    return plain(tokens, proj_in, proj_out)
+
+
 def solution(mesh):
     in_specs = (P("col", "row", None), P("col", None), P(None, "row"))
     out_specs = P("col", "row", None)
-    return jax.shard_map(shards, mesh=mesh, in_specs=in_specs, out_specs=out_specs, check_vma=False)
+    body = functools.partial(shards, mesh.shape["row"], mesh.shape["col"])
+    return jax.shard_map(body, mesh=mesh, in_specs=in_specs, out_specs=out_specs, check_vma=False)

time: 115 us -> 45.7 us (0.40)
  waiting for transfers between devices: 40.3 us -> 0 us
  Pallas kernels: 0 us -> 37.2 us
  blocking collectives: 19.8 us -> 0 us
  other arithmetic: 17.1 us -> 0 us
  between operations: 13.6 us -> 0.02 us
  matrix products: 10 us -> 0 us
  starting transfers between devices: 6.84 us -> 0 us
    pallas_call x0 -> x1, Pallas kernels: none -> 37.2 us  [fused(): pl.pallas_call(functools.partial(kernel, ways, cores, groups), out_shape=...]
    all_to_all x1 -> x0, waiting for transfers between devices: 24.7 us -> none  [shards(): lax.all_to_all(stacked, 'row', split_axis=1, concat_axis=3, tiled=True)]
    all_to_all x1 -> x0, blocking collectives: 19.8 us -> none  [shards(): lax.all_to_all(outgoing, 'row', split_axis=2, concat_axis=0, tiled=True)]
    unnamed x1 -> x0, other arithmetic: 17 us -> none
    all_gather x2 -> x0, waiting for transfers between devices: 14.2 us -> none  [the longest x1 14.2 us: shards(): lax.all_gather(proj_in, 'col', axis=0, tiled=True)]
    dot_general x10 -> x0, matrix products: 10 us -> none  [the longest x1 3.08 us: shards(): lax.dot_general(mixed, lax.all_gather(proj_out, 'row', axis=1, tiled=True...]
    all_to_all x1 -> x0, starting transfers between devices: 6.8 us -> none  [shards(): lax.all_to_all(stacked, 'row', split_axis=1, concat_axis=3, tiled=True)]
    unnamed x5 -> x13, local copies, waits for them, and re-layouts: 2.13 us -> 7.61 us
  transfers between devices with their start and end apart: 3 -> 0, of which waited for: 2 -> 0; matrix products, arithmetic and copies ran while one was open for 27% -> 0% of each run, Pallas kernels for 0% -> 0%
where the time goes in v1:
time: 45.7 us; the launch traced here: 44.9 us
  Pallas kernels  37.2 us (81%)
  local copies, waits for them, and re-layouts  7.61 us (17%)
    pallas_call x1, Pallas kernels, fused(): pl.pallas_call(functools.partial(kernel, ways, cores, groups), out_shape=...  37.2 us
    unnamed x13, local copies, waits for them, and re-layouts  7.61 us

profile of v1, /device:TPU:0, one launch (start us, length us, event | category | flops | bytes accessed | tf_op | source)
XLA Modules:
  0.0 44.9 jit_solution(7895591597377887060)
XLA Ops:
  0.0 0.0 copy-start
  0.0 1.7 %copy-done = bf16[3072,384]{1,0:T(8,128)(2,1)S(1)} copy-done((bf16[3072,384]{1,0:T(8,128)(2,1)S(1)}, bf16[3072,384]{1,0:T(8,128)(2,1)}, u32[]{:S(2)}) %copy-start) | copy-done | bytes 2359320
  1.7 0.0 copy-start.1
  1.7 1.2 %copy-done.1 = bf16[1024,512]{1,0:T(8,128)(2,1)S(1)} copy-done((bf16[1024,512]{1,0:T(8,128)(2,1)S(1)}, bf16[1024,512]{1,0:T(8,128)(2,1)}, u32[]{:S(2)}) %copy-start.1) | copy-done | bytes 1048600
  2.9 0.0 copy-start.2
  2.9 1.1 %copy-done.2 = bf16[1,192,2048]{2,1,0:T(8,128)(2,1)S(1)} copy-done((bf16[1,192,2048]{2,1,0:T(8,128)(2,1)S(1)}, bf16[1,192,2048]{2,1,0:T(8,128)(2,1)}, u32[]{:S(2)}) %copy-start.2) | copy-done | bytes 786456
  4.0 0.0 copy-start.3
  4.0 0.9 %copy-done.3 = bf16[512,128]{1,0:T(8,128)(2,1)S(1)} copy-done((bf16[512,128]{1,0:T(8,128)(2,1)S(1)}, bf16[512,128]{1,0:T(8,128)(2,1)}, u32[]{:S(2)}) %copy-start.3) | copy-done | bytes 131096
  4.9 0.0 copy-start.4
  4.9 0.9 %copy-done.4 = bf16[512,128]{1,0:T(8,128)(2,1)S(1)} copy-done((bf16[512,128]{1,0:T(8,128)(2,1)S(1)}, bf16[512,128]{1,0:T(8,128)(2,1)}, u32[]{:S(2)}) %copy-start.4) | copy-done | bytes 131096
  5.8 0.0 copy-start.5
  5.8 0.9 %copy-done.5 = bf16[128,512]{1,0:T(8,128)(2,1)S(1)} copy-done((bf16[128,512]{1,0:T(8,128)(2,1)S(1)}, bf16[128,512]{1,0:T(8,128)(2,1)}, u32[]{:S(2)}) %copy-start.5) | copy-done | bytes 131096
  6.7 37.2 %shard_map.64 = bf16[1,192,2048]{2,1,0:T(8,128)(2,1)S(1)} custom-call(bf16[1,192,2048]{2,1,0:T(8,128)(2,1)S(1)} %copy-done.2, bf16[1024,512]{1,0:T(8,128)(2,1)S(1)} %copy-done.1, bf16[512,128]{1,0:T(8,128)(2,1)S(1)} %copy-done.3, bf16[128,512]{1,0:T(8,128)(2,1)S(1)} %copy-done.5, bf16[512,128]{1,0:T(8,128)(2,1)S(1)} %copy-done.4, bf16[3072,384]{1,0:T(8,128)(2,1)S(1)} %copy-done), custom_call_target="tpu_custom_call" | custom-call | tf_op jit(solution)/shard_map/pallas_call | solution.py:418
  44.0 0.9 %copy.8 = bf16[1,192,2048]{2,1,0:T(8,128)(2,1)} copy(bf16[1,192,2048]{2,1,0:T(8,128)(2,1)S(1)} %shard_map.64) | data formatting | bytes 1572864
Async XLA Ops:
  0.0 1.7 %copy-start = (bf16[3072,384]{1,0:T(8,128)(2,1)S(1)}, bf16[3072,384]{1,0:T(8,128)(2,1)}, u32[]{:S(2)}) copy-start(bf16[3072,384]{1,0:T(8,128)(2,1)} %constant.8.clone.turn_h) | copy-start | bytes 7077892
  1.7 1.2 %copy-start.1 = (bf16[1024,512]{1,0:T(8,128)(2,1)S(1)}, bf16[1024,512]{1,0:T(8,128)(2,1)}, u32[]{:S(2)}) copy-start(bf16[1024,512]{1,0:T(8,128)(2,1)} %pin_h.1) | copy-start | bytes 3145732
  2.9 1.1 %copy-start.2 = (bf16[1,192,2048]{2,1,0:T(8,128)(2,1)S(1)}, bf16[1,192,2048]{2,1,0:T(8,128)(2,1)}, u32[]{:S(2)}) copy-start(bf16[1,192,2048]{2,1,0:T(8,128)(2,1)} %tok_h.1) | copy-start | bytes 2359300
  4.0 0.9 %copy-start.3 = (bf16[512,128]{1,0:T(8,128)(2,1)S(1)}, bf16[512,128]{1,0:T(8,128)(2,1)}, u32[]{:S(2)}) copy-start(bf16[512,128]{1,0:T(8,128)(2,1)} %pout_h.1) | copy-start | bytes 393220
  4.9 0.9 %copy-start.4 = (bf16[512,128]{1,0:T(8,128)(2,1)S(1)}, bf16[512,128]{1,0:T(8,128)(2,1)}, u32[]{:S(2)}) copy-start(bf16[512,128]{1,0:T(8,128)(2,1)} %constant.7.clone.gather_h) | copy-start | bytes 393220
  5.8 0.9 %copy-start.5 = (bf16[128,512]{1,0:T(8,128)(2,1)S(1)}, bf16[128,512]{1,0:T(8,128)(2,1)}, u32[]{:S(2)}) copy-start(bf16[128,512]{1,0:T(8,128)(2,1)} %constant.6.clone.spread_h) | copy-start | bytes 393220

commit v2 on v1

--- a/solution.py
+++ b/solution.py
@@ -209,8 +209,6 @@
         copy = load(tok_h.at[0, :, at], tok.at[m])
         if m == 0:
             first.append(copy)
-        else:
-            later_tok = copy if m == 1 else later_tok
     rest_tok = loads[2:]
     own_out = load(pout_h, wide.at[:, own_columns(row)])
     load_spread = load(spread_h, spread)
@@ -246,47 +244,48 @@
     if len(bits) >= 2:
         odd = lax.rem(col, 2)
         bits = bits[:-2] + [1 + odd, 2 - odd]
+    steps = len(bits)
     blocks = [row]
+    for bit in bits:
+        blocks = blocks + [flipped(b, bit) for b in blocks]
     my_rows = pl.ds(pl.multiple_of(col * share, TILE), share)
     ag_copies = {}
     fw_copies = []
 
-    def gather_step(step):
-        for at in range(2**step):
-            place = wide.at[my_rows, own_columns(blocks[at])]
-            slot = at + 2**step
-            copy = pltpu.make_async_remote_copy(
-                place, place, ag_send.at[slot], ag_recv.at[slot],
-                device_id={"row": flipped(row, bits[step])},
+    def land(at):
+        ag_copies[at].wait_recv()
+        for m in range(1, cores):
+            theirs = pl.ds(pl.multiple_of(core(m) * share, TILE), share)
+            ours = wide.at[my_rows, own_columns(blocks[at])]
+            other = wide.at[theirs, own_columns(blocks[at])]
+            put = pltpu.make_async_remote_copy(
+                ours, ours, fw_send.at[at, m - 1], fw_recv.at[at, cores - m - 1],
+                device_id={"col": core(m)},
             )
-            copy.start()
-            ag_copies[slot] = copy
-        blocks.extend([flipped(b, bits[step]) for b in blocks])
-
-    def gather_land(step):
-        for at in range(2**step, 2 ** (step + 1)):
-            ag_copies[at].wait_recv()
-            for m in range(1, cores):
+            put.start()
+            get = pltpu.make_async_remote_copy(
+                other, other, fw_send.at[at, m - 1], fw_recv.at[at, m - 1],
+                device_id={"col": core(m)},
+            )
+            fw_copies.append((put, get))
+
+    def level(count):
+        for at in range(ways):
+            if at.bit_count() != count:
+                continue
+            if count:
+                land(at)
+            for step in range(at.bit_length(), steps):
                 place = wide.at[my_rows, own_columns(blocks[at])]
-                theirs = wide.at[
-                    pl.ds(pl.multiple_of(core(m) * share, TILE), share), own_columns(blocks_of(m)[at])
-                ]
-                put = pltpu.make_async_remote_copy(
-                    place, place, fw_send.at[at, m - 1], fw_recv.at[at, cores - m - 1],
-                    device_id={"col": core(m)},
+                slot = at + 2**step
+                copy = pltpu.make_async_remote_copy(
+                    place, place, ag_send.at[slot], ag_recv.at[slot],
+                    device_id={"row": flipped(row, bits[step])},
                 )
-                put.start()
-                get = pltpu.make_async_remote_copy(
-                    theirs, theirs, fw_send.at[at, m - 1], fw_recv.at[at, m - 1],
-                    device_id={"col": core(m)},
-                )
-                fw_copies.append((put, get))
-
-    def blocks_of(m):
-        return blocks
-
-    steps = len(bits)
-    gather_step(0)
+                copy.start()
+                ag_copies[slot] = copy
+
+    level(0)
 
     for copy in rest_tok[: cores - 1]:
         copy.wait()
@@ -322,14 +321,10 @@
         return copies
 
     copies1 = exchange(send1, recv1, 0)
-    for step in range(steps - 2):
-        gather_land(step)
-        gather_step(step + 1)
+    level(1)
     for copy in copies1:
         copy.wait_recv()
-    if steps >= 2:
-        gather_land(steps - 2)
-        gather_step(steps - 1)
+    level(2)
 
     lane = lax.broadcasted_iota(jnp.int32, (1, LANES), 1) % slots
     lone = jnp.logical_and(lax.rem(row, quads) == 0, lane == half)
@@ -362,6 +357,8 @@
     for r in range(ways):
         send2[r] = outer[r * rows : (r + 1) * rows, :].astype(jnp.bfloat16)
     copies2 = exchange(send2, recv2, 1)
+    for count in range(3, steps):
+        level(count)
 
     load_gather.wait()
     row_part = lax.broadcasted_iota(jnp.int32, (quads * LANES, GRP), 0) // slots % pack
@@ -379,7 +376,7 @@
             jnp.concatenate([made[:, t * GRP : (t + 1) * GRP] for t in range(pack)], 0)
         )
     mixed = jnp.concatenate(columns, 1)
-    gather_land(steps - 1)
+    level(steps)
     for _, get in fw_copies:
         get.wait_recv()
 
@@ -412,9 +409,8 @@
     rows = local_len // pack
     consts = [jnp.asarray(t) for t in tables(ways, local_len, groups)]
     bf, f32 = jnp.bfloat16, jnp.float32
-    steps = ways
     dma = pltpu.SemaphoreType.DMA
-    anywhere = pl.BlockSpec(memory_space=pl.ANY)
+    anywhere = pl.BlockSpec(memory_space=pltpu.HBM)
     return pl.pallas_call(
         functools.partial(kernel, ways, cores, groups),
         out_shape=jax.ShapeDtypeStruct(tokens.shape, bf),
@@ -447,7 +443,7 @@
             dma((ways, cores)),
         ],
         compiler_params=pltpu.CompilerParams(
-            collective_id=0, has_side_effects=True, vmem_limit_bytes=48 * 2**20
+            collective_id=0, has_side_effects=True, vmem_limit_bytes=67043328
         ),
     )(tokens, proj_in, proj_out, *consts)
 

time: 45.7 us -> 29.4 us (0.64); the launches traced: 44.9 us -> 29.1 us
  Pallas kernels: 37.2 us -> 27 us
  local copies, waits for them, and re-layouts: 7.61 us -> 2.09 us
    pallas_call x1, Pallas kernels: 37.2 us -> 27 us  [fused(): pl.pallas_call(functools.partial(kernel, ways, cores, groups), out_shape=...]
    unnamed x13 -> x1, local copies, waits for them, and re-layouts: 7.61 us -> 2.09 us
where the time goes in v2:
time: 29.4 us; the launch traced here: 29.1 us
  Pallas kernels  27 us (92%)
  local copies, waits for them, and re-layouts  2.09 us (7%)
    pallas_call x1, Pallas kernels, fused(): pl.pallas_call(functools.partial(kernel, ways, cores, groups), out_shape=...  27 us
    unnamed x1, local copies, waits for them, and re-layouts  2.09 us

profile of v2, /device:TPU:0, one launch (start us, length us, event | category | flops | bytes accessed | tf_op | source)
XLA Modules:
  0.0 29.1 jit_solution(3032879792198144163)
XLA Ops:
  0.0 27.0 %shard_map.64 = bf16[1,192,2048]{2,1,0:T(8,128)(2,1)} custom-call(bf16[1,192,2048]{2,1,0:T(8,128)(2,1)} %tok_h.1, bf16[1024,512]{1,0:T(8,128)(2,1)} %pin_h.1, bf16[512,128]{1,0:T(8,128)(2,1)} %pout_h.1, bf16[128,512]{1,0:T(8,128)(2,1)} %constant.6.clone.spread_h, bf16[512,128]{1,0:T(8,128)(2,1)} %constant.7.clone.gather_h, ...), custom_call_target="tpu_custom_call" | custom-call | tf_op jit(solution)/shard_map/pallas_call | solution.py:414
  27.0 2.1 %copy.8 = bf16[1,192,2048]{2,1,0:T(8,128)(2,1)} copy(bf16[1,192,2048]{2,1,0:T(8,128)(2,1)} %shard_map.64) | data formatting | bytes 1572864

commit v3 on v2

--- a/solution.py
+++ b/solution.py
@@ -12,6 +12,7 @@
 GRP = 128
 LANES = 128
 TILE = 16
+PARTS = 4
 
 
 highest = lax.Precision.HIGHEST
@@ -170,11 +171,15 @@
     return index + bit - 2 * bit * ((index // bit) % 2)
 
 
+def partners(index, ways):
+    return [(m, lax.rem(index + m, ways)) for m in range(1, ways)]
+
+
 def kernel(
     ways, cores, groups,
-    tok_h, pin_h, pout_h, spread_h, gather_h, turn_h, out_h,
-    tok, pin, wide, spread, gather, turn, acc, send1, recv1, spec, outer, send2, recv2, res,
-    load_sem, out_sem, pin_send, pin_recv, ex_send, ex_recv, ag_send, ag_recv, fw_send, fw_recv,
+    tok_h, pin_h, pout_h, spread_h, gather_h, turn_h, mixed_v, wide,
+    tok, pin, spread, gather, turn, acc, send1, recv1, spec, outer, send2, recv2,
+    load_sem, pin_send, pin_recv, ex_send, ex_recv, ag_send, ag_recv, fw_send, fw_recv,
 ):
     row = lax.axis_index("row")
     col = lax.axis_index("col")
@@ -192,6 +197,13 @@
     def core(m):
         return lax.rem(col + m, cores)
 
+    peers = partners(row, ways)
+    barrier = pltpu.get_barrier_semaphore()
+    for _, to in peers:
+        pl.semaphore_signal(barrier, inc=1, device_id={"row": to})
+    for m in range(1, cores):
+        pl.semaphore_signal(barrier, inc=1, device_id={"col": core(m)})
+
     loads = []
 
     def load(src, dst):
@@ -215,12 +227,6 @@
     load_turn = load(turn_h, turn)
     load_gather = load(gather_h, gather)
 
-    barrier = pltpu.get_barrier_semaphore()
-    for m in range(1, ways):
-        pl.semaphore_signal(barrier, inc=1, device_id={"row": lax.rem(row + m, ways)})
-    for m in range(1, cores):
-        pl.semaphore_signal(barrier, inc=1, device_id={"col": core(m)})
-
     for copy in first:
         copy.wait()
     acc[...] = jnp.dot(tok[0], pin[0], preferred_element_type=jnp.float32)
@@ -228,13 +234,17 @@
     pl.semaphore_wait(barrier, ways - 1 + cores - 1)
 
     pin_copies = []
+    part = depth // PARTS
     for m in range(1, cores):
-        copy = pltpu.make_async_remote_copy(
-            pin.at[0], pin.at[cores - m], pin_send.at[m - 1], pin_recv.at[cores - m - 1],
-            device_id={"col": core(m)},
-        )
-        copy.start()
-        pin_copies.append(copy)
+        for at in range(PARTS):
+            span = pl.ds(at * part, part)
+            copy = pltpu.make_async_remote_copy(
+                pin.at[0, span], pin.at[cores - m, span],
+                pin_send.at[m - 1, at], pin_recv.at[cores - m - 1, at],
+                device_id={"col": core(m)},
+            )
+            copy.start()
+            pin_copies.append(copy)
 
     bits = []
     bit = ways // 2
@@ -291,8 +301,10 @@
         copy.wait()
     total = acc[...]
     for m in range(1, cores):
-        pin_copies[cores - 1 - m].wait_recv()
-        total = total + jnp.dot(tok[m], pin[m], preferred_element_type=jnp.float32)
+        for at in range(PARTS):
+            span = slice(at * part, (at + 1) * part)
+            pin_copies[(cores - 1 - m) * PARTS + at].wait_recv()
+            total = total + jnp.dot(tok[m, :, span], pin[m, span], preferred_element_type=jnp.float32)
     mapped = total.astype(jnp.bfloat16)
     load_spread.wait()
     lane_part = lax.broadcasted_iota(jnp.int32, (GRP, quads * LANES), 1) // slots % pack
@@ -309,8 +321,7 @@
 
     def exchange(src, dst, phase):
         copies = []
-        for m in range(1, ways):
-            to = lax.rem(row + m, ways)
+        for m, to in peers:
             copy = pltpu.make_async_remote_copy(
                 src.at[to], dst.at[row], ex_send.at[phase, m], ex_recv.at[phase, m],
                 device_id={"row": to},
@@ -380,21 +391,23 @@
     for _, get in fw_copies:
         get.wait_recv()
 
-    model = wide.shape[1]
-    chunk = min(512, model)
-    stores = []
-    for at in range(model // chunk):
-        span = slice(at * chunk, (at + 1) * chunk)
-        res[:, span] = jnp.dot(mixed, wide[:, span], preferred_element_type=jnp.float32).astype(
-            jnp.bfloat16
-        )
-        copy = pltpu.make_async_copy(res.at[:, span], out_h.at[0, :, span], out_sem.at[at])
-        copy.start()
-        stores.append(copy)
+    mixed_v[...] = mixed
     for copy in copies1 + copies2 + pin_copies + list(ag_copies.values()):
         copy.wait_send()
     for put, _ in fw_copies:
         put.wait_send()
+
+
+def output_map(chunk, mixed, wide, out_h, res, out_sem):
+    stores = []
+    for at in range(wide.shape[1] // chunk):
+        span = slice(at * chunk, (at + 1) * chunk)
+        res[:, span] = jnp.dot(
+            mixed[...], wide[:, span], preferred_element_type=jnp.float32
+        ).astype(jnp.bfloat16)
+        copy = pltpu.make_async_copy(res.at[:, span], out_h.at[0, :, span], out_sem.at[at])
+        copy.start()
+        stores.append(copy)
     for copy in stores:
         copy.wait()
 
@@ -411,15 +424,14 @@
     bf, f32 = jnp.bfloat16, jnp.float32
     dma = pltpu.SemaphoreType.DMA
     anywhere = pl.BlockSpec(memory_space=pltpu.HBM)
-    return pl.pallas_call(
+    mixed, wide = pl.pallas_call(
         functools.partial(kernel, ways, cores, groups),
-        out_shape=jax.ShapeDtypeStruct(tokens.shape, bf),
+        out_shape=(pltpu.VMEM((local_len, features), bf), pltpu.VMEM((features, model), bf)),
         in_specs=[anywhere] * 6,
-        out_specs=anywhere,
+        out_specs=(pl.BlockSpec(memory_space=pltpu.VMEM),) * 2,
         scratch_shapes=[
             pltpu.VMEM((cores, local_len, depth), bf),
             pltpu.VMEM((cores, depth, features), bf),
-            pltpu.VMEM((features, model), bf),
             pltpu.VMEM(consts[0].shape, bf),
             pltpu.VMEM(consts[1].shape, bf),
             pltpu.VMEM(consts[2].shape, bf),
@@ -430,11 +442,9 @@
             pltpu.VMEM((ways * rows, LANES), f32),
             pltpu.VMEM((ways, rows, LANES), bf),
             pltpu.VMEM((ways, rows, LANES), bf),
-            pltpu.VMEM((local_len, model), bf),
             dma((cores + 5,)),
-            dma((max(1, model // 512),)),
-            dma((cores,)),
-            dma((cores,)),
+            dma((cores, PARTS)),
+            dma((cores, PARTS)),
             dma((2, ways)),
             dma((2, ways)),
             dma((ways,)),
@@ -443,9 +453,18 @@
             dma((ways, cores)),
         ],
         compiler_params=pltpu.CompilerParams(
-            collective_id=0, has_side_effects=True, vmem_limit_bytes=67043328
+            collective_id=0, has_side_effects=True, vmem_limit_bytes=32 * 2**20
         ),
-    )(tokens, proj_in, proj_out, *consts)
+    )(*[pltpu.with_memory_space_constraint(x, pltpu.HBM) for x in (tokens, proj_in, proj_out, *consts)])
+    chunk = 512
+    return pl.pallas_call(
+        functools.partial(output_map, chunk),
+        out_shape=jax.ShapeDtypeStruct(tokens.shape, bf),
+        in_specs=[pl.BlockSpec(memory_space=pltpu.VMEM)] * 2,
+        out_specs=anywhere,
+        scratch_shapes=[pltpu.VMEM((local_len, model), bf), dma((model // chunk,))],
+        compiler_params=pltpu.CompilerParams(vmem_limit_bytes=16 * 2**20),
+    )(mixed, wide)
 
 
 def shards(ways, cores, tokens, proj_in, proj_out):
@@ -465,7 +484,7 @@
         and local_len % pack == 0
         and (local_len // pack) % max(ways, TILE) == 0
         and width % LANES == 0
-        and depth % LANES == 0
+        and depth % (LANES * PARTS) == 0
         and model % 512 == 0
         and features % (cores * TILE) == 0
     )

time: 29.4 us -> 27.3 us (0.929)
  local copies, waits for them, and re-layouts: 2.09 us -> 0 us
    unnamed x1 -> x0, local copies, waits for them, and re-layouts: 2.09 us -> none
    pallas_call x0 -> x1, Pallas kernels: none -> 1.3 us  [fused(): pl.pallas_call(functools.partial(output_map, chunk), out_shape=jax.ShapeD...]
    pallas_call x1, Pallas kernels: 27 us -> 25.9 us  [fused(): pl.pallas_call(functools.partial(kernel, ways, cores, groups), out_shape=...]
where the time goes in v3:
time: 27.3 us; the launch traced here: 27.2 us
  Pallas kernels  27.2 us (100%)
    pallas_call x1, Pallas kernels, fused(): pl.pallas_call(functools.partial(kernel, ways, cores, groups), out_shape=...  25.9 us
    pallas_call x1, Pallas kernels, fused(): pl.pallas_call(functools.partial(output_map, chunk), out_shape=jax.ShapeD...  1.3 us

profile of v3, /device:TPU:0, one launch (start us, length us, event | category | flops | bytes accessed | tf_op | source)
XLA Modules:
  0.0 27.2 jit_solution(10249717031514954428)
XLA Ops:
  0.0 25.9 %shard_map.64 = (bf16[192,512]{1,0:T(8,128)(2,1)S(1)}, bf16[512,2048]{1,0:T(8,128)(2,1)S(1)}) custom-call(bf16[1,192,2048]{2,1,0:T(8,128)(2,1)} %tok_h.1, bf16[1024,512]{1,0:T(8,128)(2,1)} %pin_h.1, bf16[512,128]{1,0:T(8,128)(2,1)} %pout_h.1, bf16[128,512]{1,0:T(8,128)(2,1)} %constant.6.clone.spread_h, bf16[512,128]{1,0:T(8,128)(2,1)} %constant.7.clone.gather_h, ...), custom_call_target="tpu_custom_call" | custom-call | tf_op jit(solution)/shard_map/pallas_call | solution.py:427
  25.9 1.3 %shard_map.65 = bf16[1,192,2048]{2,1,0:T(8,128)(2,1)} custom-call(bf16[192,512]{1,0:T(8,128)(2,1)S(1)} %get-tuple-element.7.mixed, bf16[512,2048]{1,0:T(8,128)(2,1)S(1)} %get-tuple-element.8.wide), custom_call_target="tpu_custom_call" | custom-call | tf_op jit(solution)/shard_map/pallas_call | solution.py:460
